TPU v7x, 32 devices: a whole 2x2x4 slice. The times are simulated.
32 devices in a mesh: tp: 8 (over z, y), dp: 4 (over x, core).
Axes of the slice: x: 2, y: 2, z: 4, core: 2. Of those that a mesh axis runs over, the one named last changes fastest.
Arguments:
- tokens: bfloat16 [128, 4096], P('dp', 'tp'), may hold values from -6 to 6
- lengths: int32 [128], P('dp'), may hold values from 1 to 96, 3072 in all
- norm_gain: float32 [2, 4096], replicated, may hold values from 0.1 to 1.9
- w_recept: bfloat16 [2, 4096, 4096], P(None, None, ('tp', 'dp')), may hold values from -0.09375 to 0.09375
- w_key: bfloat16 [2, 4096, 4096], P(None, None, ('tp', 'dp')), may hold values from -0.09375 to 0.09375
- w_value: bfloat16 [2, 4096, 4096], P(None, None, ('tp', 'dp')), may hold values from -0.09375 to 0.09375
- w_decay: bfloat16 [2, 4096, 4096], P(None, None, ('tp', 'dp')), may hold values from -0.09375 to 0.09375
- w_rate: bfloat16 [2, 4096, 4096], P(None, None, ('tp', 'dp')), may hold values from -0.09375 to 0.09375
- w_gate: bfloat16 [2, 4096, 4096], P(None, None, ('tp', 'dp')), may hold values from -0.09375 to 0.09375
- w_out: bfloat16 [2, 4096, 4096], P(None, None, ('tp', 'dp')), may hold values from -0.09375 to 0.09375
- decay_base: float32 [2, 4096], P(None, 'tp'), may hold values from -3 to 1
- rate_base: float32 [2, 4096], P(None, 'tp'), may hold values from -3 to 3
- group_gain: float32 [2, 4096], P(None, 'tp'), may hold values from 0.1 to 1.9
- state: float32 [2, 128, 64, 64, 64], P(None, 'dp', 'tp'), may hold values from -6 to 6
Outputs:
- mixed: bfloat16 [128, 4096], P('dp', 'tp')
- new_state: float32 [2, 128, 64, 64, 64], P(None, 'dp', 'tp')
Inputs may be any that keep to these rules, and one draw needn't show every extreme that they name: Each sequence's live length lies between 1 and 96, some sequences reach 96, and the lengths sum to 3072.
All inputs are finite; a program needn't handle non-finite values.
Results may differ from a plain program's by a relative error of at most 0.025.
Values may be sent and summed in bfloat16 or wider, within the bound.
A program may use at most 128 MiB of HBM per device.

v0:
```python
import jax
import jax.numpy as jnp
from jax import lax
from jax.sharding import PartitionSpec as P

STEP = 16
RMS_EPS = 1e-06
GROUP_EPS = 0.00064


def as_sent(value):

    def short(part):
        return part.astype(jnp.bfloat16) if part.dtype == jnp.float32 else part

    return jax.tree.map(short, value)


def taken_in(section, axis, dim, hop, start):

    def gathered(part):
        return lax.all_gather(part, axis, axis=dim, tiled=True)

    return hop(start, jax.tree.map(gathered, section), jnp.int32(0))


def recur(state_old, recept, key_vec, value_vec, decay_rate, learn_rate, active, head_size):
    split = (recept.shape[0], -1, head_size)
    recept_h = recept.reshape(split)
    key_h = key_vec.reshape(split)
    value_h = value_vec.reshape(split)
    decay_h = decay_rate.reshape(split)
    rate_h = learn_rate.reshape(split)
    key_len = jnp.sqrt(jnp.sum(key_h * key_h, axis=-1, keepdims=True))
    key_unit = key_h / jnp.maximum(key_len, 1e-12)
    state_a = jnp.einsum("bhij,bhj->bhi", state_old, -key_unit, precision=lax.Precision.HIGHEST)
    updated = (
        state_old * decay_h[:, :, None, :]
        + state_a[:, :, :, None] * (key_unit * rate_h)[:, :, None, :]
        + value_h[:, :, :, None] * (key_h * rate_h)[:, :, None, :]
    )
    updated = jnp.where(active[:, None, None, None], updated, state_old)
    readout = jnp.einsum("bhij,bhj->bhi", updated, recept_h, precision=lax.Precision.HIGHEST)
    centre = jnp.mean(readout, axis=-1, keepdims=True)
    spread = jnp.mean(jnp.square(readout - centre), axis=-1, keepdims=True)
    normal_out = ((readout - centre) * lax.rsqrt(spread + GROUP_EPS)).reshape(recept.shape[0], -1)
    return (updated, normal_out)


def on_device(
    tokens,
    lengths,
    norm_gain,
    w_recept,
    w_key,
    w_value,
    w_decay,
    w_rate,
    w_gate,
    w_out,
    decay_base,
    rate_base,
    group_gain,
    state,
):
    slim = w_recept.shape[2]
    head_size = state.shape[-1]
    active = lengths > STEP
    current = tokens
    updated_states = []
    for layer_idx in range(2):
        joined = jnp.concatenate(
            [
                w_recept[layer_idx],
                w_key[layer_idx],
                w_value[layer_idx],
                w_decay[layer_idx],
                w_rate[layer_idx],
                w_gate[layer_idx],
            ],
            axis=1,
        )
        batch_raw = lax.all_gather(current, "dp", axis=0, tiled=True)
        every_feature = lax.all_gather(batch_raw, "tp", axis=1, tiled=True)
        values = every_feature.astype(jnp.float32)
        factor = lax.rsqrt(jnp.mean(values * values, axis=1, keepdims=True) + RMS_EPS)
        normed = (values * factor * norm_gain[layer_idx]).astype(jnp.bfloat16)
        projected = jnp.dot(normed, joined, preferred_element_type=jnp.float32)
        pieces = [
            projected[:, idx * slim : (idx + 1) * slim].astype(jnp.bfloat16) for idx in range(6)
        ]
        arrived = (
            lax.all_to_all(as_sent(pieces[0]), "dp", split_axis=0, concat_axis=1, tiled=True),
            lax.all_to_all(as_sent(pieces[1]), "dp", split_axis=0, concat_axis=1, tiled=True),
            lax.all_to_all(as_sent(pieces[2]), "dp", split_axis=0, concat_axis=1, tiled=True),
            lax.all_to_all(as_sent(pieces[3]), "dp", split_axis=0, concat_axis=1, tiled=True),
            lax.all_to_all(as_sent(pieces[4]), "dp", split_axis=0, concat_axis=1, tiled=True),
            lax.all_to_all(as_sent(pieces[5]), "dp", split_axis=0, concat_axis=1, tiled=True),
        )
        recept, key_vec, value_vec, decay_pre, rate_pre, gate_pre = [
            item.astype(jnp.float32) for item in arrived
        ]
        decay_rate = jnp.exp(-jnp.exp(-jax.nn.softplus(-(decay_base[layer_idx] + decay_pre)) - 0.5))
        learn_rate = jax.nn.sigmoid(rate_base[layer_idx] + rate_pre)
        gate_open = jax.nn.sigmoid(gate_pre)
        updated, normal_out = recur(
            state[layer_idx], recept, key_vec, value_vec, decay_rate, learn_rate, active, head_size
        )
        updated_states.append(updated)
        mixed_here = jnp.where(
            active[:, None], normal_out * group_gain[layer_idx] * gate_open, 0.0
        ).astype(jnp.bfloat16)
        rows_all = lax.all_gather(mixed_here, "dp", axis=0, tiled=True)
        out_weight = w_out[layer_idx]

        def fold_output(acc_sum, segment, offset):
            weight_rows = lax.dynamic_slice_in_dim(out_weight, offset, segment.shape[1], 0)
            return acc_sum + jnp.dot(segment, weight_rows, preferred_element_type=jnp.float32)

        blank = jnp.zeros((rows_all.shape[0], out_weight.shape[1]), jnp.float32)
        out_cols = taken_in(rows_all, "tp", 1, fold_output, blank).astype(jnp.bfloat16)
        current = lax.all_to_all(out_cols, "dp", split_axis=0, concat_axis=1, tiled=True)
    return (current, jnp.stack(updated_states))


def solution(mesh):
    in_specs = (
        P("dp", "tp"),
        P("dp"),
        P(),
        P(None, None, ("tp", "dp")),
        P(None, None, ("tp", "dp")),
        P(None, None, ("tp", "dp")),
        P(None, None, ("tp", "dp")),
        P(None, None, ("tp", "dp")),
        P(None, None, ("tp", "dp")),
        P(None, None, ("tp", "dp")),
        P(None, "tp"),
        P(None, "tp"),
        P(None, "tp"),
        P(None, "dp", "tp", None, None),
    )
    out_specs = (P("dp", "tp"), P(None, "dp", "tp", None, None))
    return jax.shard_map(
        on_device, mesh=mesh, in_specs=in_specs, out_specs=out_specs, check_vma=False
    )
```

profile of v0, /device:TPU:0, one launch (start us, length us, event | category | flops | bytes accessed | tf_op | source)
XLA Modules:
  0.0 369.8 jit_solution(15429060833024685349)
XLA Ops:
  7.2 8.5 %all_gather.24 = bf16[128,512]{1,0:T(8,128)(2,1)} all-gather(bf16[32,512]{1,0:T(8,128)(2,1)} %param.14), channel_id=1, replica_groups=mesh['tp'=8,'dp'=4] {'dp'}, dimensions={0}, use_global_device_ids=true | all-gather | bytes 163840 | tf_op jit(solution)/shard_map/all_gather | solution.py:83
  16.5 3.2 bitcast_dynamic-update-slice_fusion.11
  19.7 3.2 bitcast_dynamic-update-slice_fusion.10
  23.0 1.5 bitcast_dynamic-update-slice_fusion.9
  24.5 1.5 bitcast_dynamic-update-slice_fusion.8
  26.0 1.5 bitcast_dynamic-update-slice_fusion.7
  27.6 1.6 bitcast_dynamic-update-slice_fusion.6
  29.2 26.5 %all-gather.5.cloned.1.call-done = bf16[128,4096]{1,0:T(8,128)(2,1)} async-done(((bf16[128,512]{1,0:T(8,128)(2,1)}), bf16[128,4096]{1,0:T(8,128)(2,1)}) %all-gather.5.cloned.1.call-update) | async-done | bytes 1048592 | tf_op jit(solution)/shard_map/all_gather | solution.py:84
  55.7 1.5 fusion.30
  57.3 4.2 %convolution_convert_fusion.1 = bf16[128,768]{1,0:T(8,128)(2,1)S(1)} fusion(bf16[4096,768]{1,0:T(8,128)(2,1)} %get-tuple-element.8, bf16[128,4096]{1,0:T(8,128)(2,1)} %all-gather.5.cloned.1.call-done, f32[4096]{0:T(1024)S(1)} %bitcast.161, f32[128]{0:T(128)S(1)} %add_rsqrt_fusion.3), kind=kOutput, calls=%fused_computation.48 | convolution fusion | flops 807501824 | bytes 7553536 | tf_op jit(solution)/shard_map/dot_general | solution.py:88
  62.1 3.3 all-to-all-start.4
  65.4 3.9 %all-to-all-done.4 = bf16[4,32,128]{2,1,0:T(8,128)(2,1)S(1)} async-done(((bf16[4,32,128]{2,1,0:T(8,128)(2,1)}), bf16[4,32,128]{2,1,0:T(8,128)(2,1)S(1)}, u32[]{:S(2)}, u32[]{:S(2)}) %all-to-all-start.4) | async-done | bytes 32800 | tf_op jit(solution)/shard_map/all_to_all | solution.py:93
  69.3 3.3 all-to-all-start.1
  72.8 3.7 %all-to-all-done.1 = bf16[4,32,128]{2,1,0:T(8,128)(2,1)S(1)} async-done(((bf16[4,32,128]{2,1,0:T(8,128)(2,1)}), bf16[4,32,128]{2,1,0:T(8,128)(2,1)S(1)}, u32[]{:S(2)}, u32[]{:S(2)}) %all-to-all-start.1) | async-done | bytes 32800 | tf_op jit(solution)/shard_map/all_to_all | solution.py:94
  76.5 3.3 all-to-all-start.2
  79.8 3.9 %all-to-all-done.2 = bf16[4,32,128]{2,1,0:T(8,128)(2,1)S(1)} async-done(((bf16[4,32,128]{2,1,0:T(8,128)(2,1)}), bf16[4,32,128]{2,1,0:T(8,128)(2,1)S(1)}, u32[]{:S(2)}, u32[]{:S(2)}) %all-to-all-start.2) | async-done | bytes 32800 | tf_op jit(solution)/shard_map/all_to_all | solution.py:97
  83.6 3.3 all-to-all-start.3
  86.9 3.9 %all-to-all-done.3 = bf16[4,32,128]{2,1,0:T(8,128)(2,1)S(1)} async-done(((bf16[4,32,128]{2,1,0:T(8,128)(2,1)}), bf16[4,32,128]{2,1,0:T(8,128)(2,1)S(1)}, u32[]{:S(2)}, u32[]{:S(2)}) %all-to-all-start.3) | async-done | bytes 32800 | tf_op jit(solution)/shard_map/all_to_all | solution.py:95
  90.8 3.3 all-to-all-start
  94.3 3.7 %all-to-all-done = bf16[4,32,128]{2,1,0:T(8,128)(2,1)S(1)} async-done(((bf16[4,32,128]{2,1,0:T(8,128)(2,1)}), bf16[4,32,128]{2,1,0:T(8,128)(2,1)S(1)}, u32[]{:S(2)}, u32[]{:S(2)}) %all-to-all-start) | async-done | bytes 32800 | tf_op jit(solution)/shard_map/all_to_all | solution.py:96
  98.0 3.3 all-to-all-start.5
  102.3 15.4 %fusion = f32[32,8,1,64]{3,2,1,0:T(1,128)S(1)} fusion(f32[32,8,64,1]{2,3,1,0:T(1,128)S(1)} %bitcast.154, f32[2,32,8,64,64]{4,3,2,1,0:T(8,128)} %param.27), kind=kOutput, calls=%fused_computation.2 | convolution fusion | flops 12582912 | bytes 8519680 | tf_op jit(solution)/shard_map/bhij,bhj->bhi/dot_general | solution.py:36
  117.7 11.1 %fusion.4 = f32[32,8,1,64]{3,2,1,0:T(1,128)S(1)} fusion(bf16[32,8,64,1]{2,3,1,0:T(2,128)(2,1)S(1)} %reshape.317, f32[2,32,8,64,64]{4,3,2,1,0:T(8,128)} %param.27, f32[32,8,64]{2,1,0:T(8,128)S(1)} %get-tuple-element.23, f32[32,8,64]{2,1,0:T(8,128)S(1)} %reshape.299, f32[32,8,64]{2,1,0:T(8,128)S(1)} %get-tuple-element.22, f32[32,8,64]{2,1,0:T(8,128)S(1)} %bitcast.150, ...), kind=kOutput, calls=%fused_computation.7 | convolution fusion | flops 18874368 | bytes 8814624 | tf_op jit(solution)/shard_map/bhij,bhj->bhi/dot_general | solution.py:43
  129.4 6.1 %all_gather.26 = bf16[128,512]{1,0:T(8,128)(2,1)} all-gather(bf16[32,512]{1,0:T(8,128)(2,1)S(1)} %fusion.59), channel_id=1, replica_groups=mesh['tp'=8,'dp'=4] {'dp'}, dimensions={0}, use_global_device_ids=true | all-gather | bytes 163840 | tf_op jit(solution)/shard_map/all_gather | solution.py:113
  135.5 38.9 %all-gather.7.cloned.1.call-done = bf16[128,4096]{1,0:T(8,128)(2,1)} async-done(((bf16[128,512]{1,0:T(8,128)(2,1)}), bf16[128,4096]{1,0:T(8,128)(2,1)}) %all-gather.7.cloned.1.call-update) | async-done | bytes 1048592 | tf_op jit(solution)/shard_map/all_gather | solution.py:22
  174.5 2.0 convolution_convert_fusion.3
  176.4 6.6 %all_to_all.200 = bf16[4,32,128]{2,1,0:T(8,128)(2,1)S(1)} all-to-all(bf16[4,32,128]{2,1,0:T(8,128)(2,1)S(1)} %bitcast.159), channel_id=1, replica_groups=mesh['tp'=8,'dp'=4] {'dp'}, dimensions={0} | all-to-all | bytes 65536 | tf_op jit(solution)/shard_map/all_to_all | solution.py:122
  183.0 5.9 %all_gather.28 = bf16[128,512]{1,0:T(8,128)(2,1)} all-gather(bf16[32,512]{1,0:T(8,128)(2,1)S(1)} %copy_bitcast_fusion.1), channel_id=1, replica_groups=mesh['tp'=8,'dp'=4] {'dp'}, dimensions={0}, use_global_device_ids=true | all-gather | bytes 163840 | tf_op jit(solution)/shard_map/all_gather | solution.py:83
  188.9 37.5 %all-gather.9.cloned.1.call-done = bf16[128,4096]{1,0:T(8,128)(2,1)} async-done(((bf16[128,512]{1,0:T(8,128)(2,1)}), bf16[128,4096]{1,0:T(8,128)(2,1)}) %all-gather.9.cloned.1.call-update) | async-done | bytes 1048592 | tf_op jit(solution)/shard_map/all_gather | solution.py:84
  228.0 4.2 %convolution_convert_fusion = bf16[128,768]{1,0:T(8,128)(2,1)S(1)} fusion(bf16[4096,768]{1,0:T(8,128)(2,1)} %get-tuple-element.9, bf16[128,4096]{1,0:T(8,128)(2,1)} %all-gather.9.cloned.1.call-done, f32[4096]{0:T(1024)S(1)} %bitcast.160, f32[128]{0:T(128)S(1)} %add_rsqrt_fusion.2), kind=kOutput, calls=%fused_computation.47 | convolution fusion | flops 807501824 | bytes 7553536 | tf_op jit(solution)/shard_map/dot_general | solution.py:88
  232.8 6.6 %all_to_all.201 = bf16[4,32,128]{2,1,0:T(8,128)(2,1)S(1)} all-to-all(bf16[4,32,128]{2,1,0:T(8,128)(2,1)S(1)} %bitcast.156), channel_id=1, replica_groups=mesh['tp'=8,'dp'=4] {'dp'}, dimensions={0} | all-to-all | bytes 65536 | tf_op jit(solution)/shard_map/all_to_all | solution.py:93
  239.4 3.3 all-to-all-start.8
  242.8 3.8 %all-to-all-done.8 = bf16[4,32,128]{2,1,0:T(8,128)(2,1)S(1)} async-done(((bf16[4,32,128]{2,1,0:T(8,128)(2,1)}), bf16[4,32,128]{2,1,0:T(8,128)(2,1)S(1)}, u32[]{:S(2)}, u32[]{:S(2)}) %all-to-all-start.8) | async-done | bytes 32800 | tf_op jit(solution)/shard_map/all_to_all | solution.py:94
  246.6 3.3 all-to-all-start.9
  249.9 3.9 %all-to-all-done.9 = bf16[4,32,128]{2,1,0:T(8,128)(2,1)S(1)} async-done(((bf16[4,32,128]{2,1,0:T(8,128)(2,1)}), bf16[4,32,128]{2,1,0:T(8,128)(2,1)S(1)}, u32[]{:S(2)}, u32[]{:S(2)}) %all-to-all-start.9) | async-done | bytes 32800 | tf_op jit(solution)/shard_map/all_to_all | solution.py:97
  253.8 3.3 all-to-all-start.10
  257.1 3.9 %all-to-all-done.10 = bf16[4,32,128]{2,1,0:T(8,128)(2,1)S(1)} async-done(((bf16[4,32,128]{2,1,0:T(8,128)(2,1)}), bf16[4,32,128]{2,1,0:T(8,128)(2,1)S(1)}, u32[]{:S(2)}, u32[]{:S(2)}) %all-to-all-start.10) | async-done | bytes 32800 | tf_op jit(solution)/shard_map/all_to_all | solution.py:95
  261.0 3.3 all-to-all-start.7
  264.4 3.7 %all-to-all-done.7 = bf16[4,32,128]{2,1,0:T(8,128)(2,1)S(1)} async-done(((bf16[4,32,128]{2,1,0:T(8,128)(2,1)}), bf16[4,32,128]{2,1,0:T(8,128)(2,1)S(1)}, u32[]{:S(2)}, u32[]{:S(2)}) %all-to-all-start.7) | async-done | bytes 32800 | tf_op jit(solution)/shard_map/all_to_all | solution.py:96
  268.1 3.3 all-to-all-start.12
  272.3 15.4 %fusion.5 = f32[32,8,1,64]{3,2,1,0:T(1,128)S(1)} fusion(f32[32,8,64,1]{2,3,1,0:T(1,128)S(1)} %bitcast.155, f32[2,32,8,64,64]{4,3,2,1,0:T(8,128)} %param.27), kind=kOutput, calls=%fused_computation.9 | convolution fusion | flops 12582912 | bytes 8519680 | tf_op jit(solution)/shard_map/bhij,bhj->bhi/dot_general | solution.py:36
  287.8 11.1 %fusion.9 = f32[32,8,1,64]{3,2,1,0:T(1,128)S(1)} fusion(bf16[32,8,64,1]{2,3,1,0:T(2,128)(2,1)S(1)} %reshape.319, f32[2,32,8,64,64]{4,3,2,1,0:T(8,128)} %param.27, f32[32,8,64]{2,1,0:T(8,128)S(1)} %get-tuple-element.21, f32[32,8,64]{2,1,0:T(8,128)S(1)} %reshape.305, f32[32,8,64]{2,1,0:T(8,128)S(1)} %get-tuple-element.20, f32[32,8,64]{2,1,0:T(8,128)S(1)} %bitcast.152, ...), kind=kOutput, calls=%fused_computation.14 | convolution fusion | flops 18874368 | bytes 8814624 | tf_op jit(solution)/shard_map/bhij,bhj->bhi/dot_general | solution.py:43
  299.5 5.9 %all_gather.30 = bf16[128,512]{1,0:T(8,128)(2,1)} all-gather(bf16[32,512]{1,0:T(8,128)(2,1)S(1)} %fusion.57), channel_id=1, replica_groups=mesh['tp'=8,'dp'=4] {'dp'}, dimensions={0}, use_global_device_ids=true | all-gather | bytes 163840 | tf_op jit(solution)/shard_map/all_gather | solution.py:113
  305.4 13.7 %add_select_fusion.1 = (f32[1,32,8,64,64]{4,3,2,1,0:T(8,128)}, f32[1,32,8,64,64]{4,3,2,1,0:T(8,128)}) fusion(f32[2,32,8,64,64]{4,3,2,1,0:T(8,128)} %param.27, f32[32,8,64]{2,1,0:T(8,128)S(1)} %get-tuple-element.23, f32[32,8,64]{2,1,0:T(8,128)S(1)} %reshape.299, f32[32,8,64]{2,1,0:T(8,128)S(1)} %get-tuple-element.22, f32[32,8,64]{2,1,0:T(8,128)S(1)} %bitcast.151, ...), kind=kLoop, calls=%fused_computation.16 | loop fusion | flops 12582912 | bytes 17432608 | tf_op jit(solution)/shard_map/jit(_where)/select_n | solution.py:42
  319.1 25.2 %all-gather.11.cloned.1.call-done = bf16[128,4096]{1,0:T(8,128)(2,1)} async-done(((bf16[128,512]{1,0:T(8,128)(2,1)}), bf16[128,4096]{1,0:T(8,128)(2,1)}) %all-gather.11.cloned.1.call-update) | async-done | bytes 1048592 | tf_op jit(solution)/shard_map/all_gather | solution.py:22
  344.3 2.6 convolution_convert_fusion.2
  346.9 3.3 all-to-all-start.13
  350.2 12.5 %pad_maximum_fusion = f32[2,32,8,64,64]{4,3,2,1,0:T(8,128)} fusion(f32[1,32,8,64,64]{4,3,2,1,0:T(8,128)} %get-tuple-element.7, f32[1,32,8,64,64]{4,3,2,1,0:T(8,128)} %get-tuple-element.6), kind=kLoop, calls=%fused_computation | loop fusion | flops 2097152 | bytes 16777216 | tf_op jit(solution)/shard_map/stack | solution.py:123
  (92 shorter events, 8.3 us)
Async XLA Ops:
  7.2 15.8 %copy-start = (bf16[2,4096,128]{2,1,0:T(8,128)(2,1)S(1)}, bf16[2,4096,128]{2,1,0:T(8,128)(2,1)}, u32[]{:S(2)}) copy-start(bf16[2,4096,128]{2,1,0:T(8,128)(2,1)} %param.19) | copy-start | bytes 6291460
  7.2 48.6 %all-gather.5.cloned.1.call-start = ((), (), s32[]{:S(2)}) async-start(), calls=%async_computation.14 | async-start | bytes 1179648 | tf_op jit(solution)/shard_map/all_gather | solution.py:84
  16.5 8.0 %copy-start.1 = (bf16[2,4096,128]{2,1,0:T(8,128)(2,1)S(1)}, bf16[2,4096,128]{2,1,0:T(8,128)(2,1)}, u32[]{:S(2)}) copy-start(bf16[2,4096,128]{2,1,0:T(8,128)(2,1)} %param.20) | copy-start | bytes 6291460
  19.7 6.3 %copy-start.2 = (bf16[2,4096,128]{2,1,0:T(8,128)(2,1)S(1)}, bf16[2,4096,128]{2,1,0:T(8,128)(2,1)}, u32[]{:S(2)}) copy-start(bf16[2,4096,128]{2,1,0:T(8,128)(2,1)} %param.21) | copy-start | bytes 6291460
  23.0 4.6 %copy-start.4 = (f32[2,4096]{1,0:T(2,128)S(1)}, f32[2,4096]{1,0:T(2,128)}, u32[]{:S(2)}) copy-start(f32[2,4096]{1,0:T(2,128)} %param.16) | copy-start | bytes 98308
  23.0 4.6 %copy-start.3 = (bf16[2,4096,128]{2,1,0:T(8,128)(2,1)S(1)}, bf16[2,4096,128]{2,1,0:T(8,128)(2,1)}, u32[]{:S(2)}) copy-start(bf16[2,4096,128]{2,1,0:T(8,128)(2,1)} %param.22) | copy-start | bytes 6291460
  27.6 37.8 %copy-start.7 = (s32[32]{0:T(128)S(1)}, s32[32]{0:T(128)}, u32[]{:S(2)}) copy-start(s32[32]{0:T(128)} %param.15) | copy-start | bytes 388
  27.6 44.9 %copy-start.5 = (f32[2,512]{1,0:T(2,128)S(1)}, f32[2,512]{1,0:T(2,128)}, u32[]{:S(2)}) copy-start(f32[2,512]{1,0:T(2,128)} %param.25) | copy-start | bytes 12292
  27.6 44.9 %copy-start.6 = (f32[2,512]{1,0:T(2,128)S(1)}, f32[2,512]{1,0:T(2,128)}, u32[]{:S(2)}) copy-start(f32[2,512]{1,0:T(2,128)} %param.24) | copy-start | bytes 12292
  62.1 7.2 %all-to-all-start.4 = ((bf16[4,32,128]{2,1,0:T(8,128)(2,1)}), bf16[4,32,128]{2,1,0:T(8,128)(2,1)S(1)}, u32[]{:S(2)}, u32[]{:S(2)}) async-start(bf16[4,32,128]{2,1,0:T(8,128)(2,1)} %bitcast.21), calls=%async_computation.4 | async-start | bytes 65536 | tf_op jit(solution)/shard_map/all_to_all | solution.py:93
  69.3 7.2 %all-to-all-start.1 = ((bf16[4,32,128]{2,1,0:T(8,128)(2,1)}), bf16[4,32,128]{2,1,0:T(8,128)(2,1)S(1)}, u32[]{:S(2)}, u32[]{:S(2)}) async-start(bf16[4,32,128]{2,1,0:T(8,128)(2,1)} %bitcast.11), calls=%async_computation.1 | async-start | bytes 65536 | tf_op jit(solution)/shard_map/all_to_all | solution.py:94
  76.5 7.2 %all-to-all-start.2 = ((bf16[4,32,128]{2,1,0:T(8,128)(2,1)}), bf16[4,32,128]{2,1,0:T(8,128)(2,1)S(1)}, u32[]{:S(2)}, u32[]{:S(2)}) async-start(bf16[4,32,128]{2,1,0:T(8,128)(2,1)} %bitcast.17), calls=%async_computation.2 | async-start | bytes 65536 | tf_op jit(solution)/shard_map/all_to_all | solution.py:97
  83.6 7.2 %all-to-all-start.3 = ((bf16[4,32,128]{2,1,0:T(8,128)(2,1)}), bf16[4,32,128]{2,1,0:T(8,128)(2,1)S(1)}, u32[]{:S(2)}, u32[]{:S(2)}) async-start(bf16[4,32,128]{2,1,0:T(8,128)(2,1)} %bitcast.19), calls=%async_computation.3 | async-start | bytes 65536 | tf_op jit(solution)/shard_map/all_to_all | solution.py:95
  90.8 7.2 %all-to-all-start = ((bf16[4,32,128]{2,1,0:T(8,128)(2,1)}), bf16[4,32,128]{2,1,0:T(8,128)(2,1)S(1)}, u32[]{:S(2)}, u32[]{:S(2)}) async-start(bf16[4,32,128]{2,1,0:T(8,128)(2,1)} %bitcast.9), calls=%async_computation | async-start | bytes 65536 | tf_op jit(solution)/shard_map/all_to_all | solution.py:96
  98.0 31.3 %all-to-all-start.5 = ((bf16[4,32,128]{2,1,0:T(8,128)(2,1)}), bf16[4,32,128]{2,1,0:T(8,128)(2,1)S(1)}, u32[]{:S(2)}, u32[]{:S(2)}) async-start(bf16[4,32,128]{2,1,0:T(8,128)(2,1)} %bitcast.26), calls=%async_computation.5 | async-start | bytes 65536 | tf_op jit(solution)/shard_map/all_to_all | solution.py:98
  101.3 73.2 %all-gather.7.cloned.1.call-start = ((), (), s32[]{:S(2)}) async-start(), calls=%async_computation.15 | async-start | bytes 1179648 | tf_op jit(solution)/shard_map/all_gather | solution.py:22
  135.5 91.0 %all-gather.9.cloned.1.call-start = ((), (), s32[]{:S(2)}) async-start(), calls=%async_computation.16 | async-start | bytes 1179648 | tf_op jit(solution)/shard_map/all_gather | solution.py:84
  239.4 7.2 %all-to-all-start.8 = ((bf16[4,32,128]{2,1,0:T(8,128)(2,1)}), bf16[4,32,128]{2,1,0:T(8,128)(2,1)S(1)}, u32[]{:S(2)}, u32[]{:S(2)}) async-start(bf16[4,32,128]{2,1,0:T(8,128)(2,1)} %bitcast.40), calls=%async_computation.8 | async-start | bytes 65536 | tf_op jit(solution)/shard_map/all_to_all | solution.py:94
  246.6 7.2 %all-to-all-start.9 = ((bf16[4,32,128]{2,1,0:T(8,128)(2,1)}), bf16[4,32,128]{2,1,0:T(8,128)(2,1)S(1)}, u32[]{:S(2)}, u32[]{:S(2)}) async-start(bf16[4,32,128]{2,1,0:T(8,128)(2,1)} %bitcast.46), calls=%async_computation.9 | async-start | bytes 65536 | tf_op jit(solution)/shard_map/all_to_all | solution.py:97
  253.8 7.2 %all-to-all-start.10 = ((bf16[4,32,128]{2,1,0:T(8,128)(2,1)}), bf16[4,32,128]{2,1,0:T(8,128)(2,1)S(1)}, u32[]{:S(2)}, u32[]{:S(2)}) async-start(bf16[4,32,128]{2,1,0:T(8,128)(2,1)} %bitcast.48), calls=%async_computation.10 | async-start | bytes 65536 | tf_op jit(solution)/shard_map/all_to_all | solution.py:95
  261.0 7.2 %all-to-all-start.7 = ((bf16[4,32,128]{2,1,0:T(8,128)(2,1)}), bf16[4,32,128]{2,1,0:T(8,128)(2,1)S(1)}, u32[]{:S(2)}, u32[]{:S(2)}) async-start(bf16[4,32,128]{2,1,0:T(8,128)(2,1)} %bitcast.38), calls=%async_computation.7 | async-start | bytes 65536 | tf_op jit(solution)/shard_map/all_to_all | solution.py:96
  268.1 31.3 %all-to-all-start.12 = ((bf16[4,32,128]{2,1,0:T(8,128)(2,1)}), bf16[4,32,128]{2,1,0:T(8,128)(2,1)S(1)}, u32[]{:S(2)}, u32[]{:S(2)}) async-start(bf16[4,32,128]{2,1,0:T(8,128)(2,1)} %bitcast.55), calls=%async_computation.12 | async-start | bytes 65536 | tf_op jit(solution)/shard_map/all_to_all | solution.py:98
  271.4 72.9 %all-gather.11.cloned.1.call-start = ((), (), s32[]{:S(2)}) async-start(), calls=%async_computation.17 | async-start | bytes 1179648 | tf_op jit(solution)/shard_map/all_gather | solution.py:22
  346.9 15.8 %all-to-all-start.13 = ((bf16[4,32,128]{2,1,0:T(8,128)(2,1)}), bf16[4,32,128]{2,1,0:T(8,128)(2,1)S(1)}, u32[]{:S(2)}, u32[]{:S(2)}) async-start(bf16[4,32,128]{2,1,0:T(8,128)(2,1)} %bitcast.58), calls=%async_computation.13 | async-start | bytes 65536 | tf_op jit(solution)/shard_map/all_to_all | solution.py:122
Sparse Core Ops, SparseCore 0:
  15.9 39.8 all-gather.4
  135.6 38.8 all-gather.6
  189.0 37.3 all-gather.8
  305.6 38.7 all-gather.10
where the time goes:
time: 371 us; the launch traced here: 370 us
  waiting for transfers between devices  163 us (44%)
  matrix products  65.7 us (18%)
  blocking collectives  39.6 us (11%)
  starting transfers between devices  39.3 us (11%)
  other arithmetic  31 us (8%)
  local copies, waits for them, and re-layouts  17.3 us (5%)
  between operations  14.3 us (4%)
    all_gather x2, waiting for transfers between devices, gathered(): return lax.all_gather(part, axis, axis=dim, tiled=True)  64.1 us
    all_gather x2, waiting for transfers between devices, on_device(): every_feature = lax.all_gather(batch_raw, 'tp', axis=1, tiled=True)  64.1 us
    dot_general x2, matrix products, recur(): jnp.einsum('bhij,bhj->bhi', state_old, -key_unit, precision=lax.Precision...  30.8 us
    dot_general x2, matrix products, recur(): jnp.einsum('bhij,bhj->bhi', updated, recept_h, precision=lax.Precision.HI...  22.1 us
    all_gather x2, blocking collectives, on_device(): batch_raw = lax.all_gather(current, 'dp', axis=0, tiled=True)  14.4 us
    select_n x1, other arithmetic, recur(): updated = jnp.where(active[:, None, None, None], updated, state_old)  13.7 us
    another operation x1, other arithmetic, on_device(): return (current, jnp.stack(updated_states))  12.5 us
    all_gather x2, blocking collectives, on_device(): rows_all = lax.all_gather(mixed_here, 'dp', axis=0, tiled=True)  12 us
  transfers between devices with their start and end apart: 16, of which 13 were waited for; matrix products, arithmetic and copies ran while one was open for 26% of the time, Pallas kernels for 0%

commit v1 on v0

--- a/solution.py
+++ b/solution.py
@@ -6,6 +6,16 @@
 STEP = 16
 RMS_EPS = 1e-06
 GROUP_EPS = 0.00064
+
+
+def turned_line(shard, mesh_axis, dim):
+    size = lax.axis_size(mesh_axis)
+    held, pieces = (shard, [shard])
+    for _ in range(size - 1):
+        held = lax.ppermute(held, mesh_axis, [(i, (i + 1) % size) for i in range(size)])
+        pieces.insert(0, held)
+    line = jnp.concatenate(pieces, axis=dim)
+    return jnp.roll(line, (lax.axis_index(mesh_axis) + 1) * shard.shape[dim], axis=dim)
 
 
 def as_sent(value):
@@ -81,7 +91,7 @@
             axis=1,
         )
         batch_raw = lax.all_gather(current, "dp", axis=0, tiled=True)
-        every_feature = lax.all_gather(batch_raw, "tp", axis=1, tiled=True)
+        every_feature = turned_line(batch_raw, "tp", 1)
         values = every_feature.astype(jnp.float32)
         factor = lax.rsqrt(jnp.mean(values * values, axis=1, keepdims=True) + RMS_EPS)
         normed = (values * factor * norm_gain[layer_idx]).astype(jnp.bfloat16)

time: 371 us -> 397 us (1.070)
  waiting for transfers between devices: 163 us -> 194 us
  local copies, waits for them, and re-layouts: 17.3 us -> 12.8 us
    ppermute x0 -> x14, waiting for transfers between devices: none -> 99.2 us  [turned_line(): lax.ppermute(held, mesh_axis, [(i, (i + 1) % size) for i in range(size)])]
    all_gather x2 -> x0, waiting for transfers between devices: 64.1 us -> none  [on_device(): every_feature = lax.all_gather(batch_raw, 'tp', axis=1, tiled=True)]
    unnamed x21 -> x41, local copies, waits for them, and re-layouts: 11.1 us -> 8.4 us
  transfers between devices with their start and end apart: 16 -> 28, of which waited for: 13 -> 25; matrix products, arithmetic and copies ran while one was open for 26% -> 22% of each run, Pallas kernels for 0% -> 0%
where the time goes in v1:
time: 397 us; the launch traced here: 396 us
  waiting for transfers between devices  194 us (49%)
  matrix products  65.7 us (17%)
  starting transfers between devices  42.5 us (11%)
  blocking collectives  36.9 us (9%)
  other arithmetic  29.3 us (7%)
  between operations  14.8 us (4%)
  local copies, waits for them, and re-layouts  12.8 us (3%)
    ppermute x14, waiting for transfers between devices, turned_line(): lax.ppermute(held, mesh_axis, [(i, (i + 1) % size) for i in range(size)])  99.2 us
    all_gather x2, waiting for transfers between devices, gathered(): return lax.all_gather(part, axis, axis=dim, tiled=True)  60.6 us
    dot_general x2, matrix products, recur(): jnp.einsum('bhij,bhj->bhi', state_old, -key_unit, precision=lax.Precision...  30.8 us
    dot_general x2, matrix products, recur(): jnp.einsum('bhij,bhj->bhi', updated, recept_h, precision=lax.Precision.HI...  22.1 us
    select_n x1, other arithmetic, recur(): updated = jnp.where(active[:, None, None, None], updated, state_old)  13.7 us
    another operation x1, other arithmetic, on_device(): return (current, jnp.stack(updated_states))  12.5 us
    all_gather x2, blocking collectives, on_device(): batch_raw = lax.all_gather(current, 'dp', axis=0, tiled=True)  12.3 us
    all_gather x2, blocking collectives, on_device(): rows_all = lax.all_gather(mixed_here, 'dp', axis=0, tiled=True)  11.8 us
  transfers between devices with their start and end apart: 28, of which 25 were waited for; matrix products, arithmetic and copies ran while one was open for 22% of the time, Pallas kernels for 0%

profile of v1, /device:TPU:0, one launch (start us, length us, event | category | flops | bytes accessed | tf_op | source)
XLA Modules:
  0.0 396.1 jit_solution(9589916346645932603)
XLA Ops:
  7.2 6.9 %all_gather.18 = bf16[128,512]{1,0:T(8,128)(2,1)S(1)} all-gather(bf16[32,512]{1,0:T(8,128)(2,1)} %param.16), channel_id=1, replica_groups=mesh['tp'=8,'dp'=4] {'dp'}, dimensions={0}, use_global_device_ids=true | all-gather | bytes 163840 | tf_op jit(solution)/shard_map/all_gather | solution.py:93
  23.5 7.4 %collective-permute-done.1 = bf16[128,512]{1,0:T(8,128)(2,1)S(1)} collective-permute-done((bf16[128,512]{1,0:T(8,128)(2,1)S(1)}, bf16[128,512]{1,0:T(8,128)(2,1)S(1)}, u32[]{:S(2)}, u32[]{:S(2)}) %collective-permute-start.1) | collective-permute-done | bytes 131104 | tf_op jit(solution)/shard_map/ppermute | solution.py:15
  31.4 7.1 %collective-permute-done.2 = bf16[128,512]{1,0:T(8,128)(2,1)S(1)} collective-permute-done((bf16[128,512]{1,0:T(8,128)(2,1)S(1)}, bf16[128,512]{1,0:T(8,128)(2,1)S(1)}, u32[]{:S(2)}, u32[]{:S(2)}) %collective-permute-start.2) | collective-permute-done | bytes 131104 | tf_op jit(solution)/shard_map/ppermute | solution.py:15
  39.0 7.2 %collective-permute-done.3 = bf16[128,512]{1,0:T(8,128)(2,1)S(1)} collective-permute-done((bf16[128,512]{1,0:T(8,128)(2,1)S(1)}, bf16[128,512]{1,0:T(8,128)(2,1)S(1)}, u32[]{:S(2)}, u32[]{:S(2)}) %collective-permute-start.3) | collective-permute-done | bytes 131104 | tf_op jit(solution)/shard_map/ppermute | solution.py:15
  49.3 4.5 %collective-permute-done.4 = bf16[128,512]{1,0:T(8,128)(2,1)S(1)} collective-permute-done((bf16[128,512]{1,0:T(8,128)(2,1)S(1)}, bf16[128,512]{1,0:T(8,128)(2,1)S(1)}, u32[]{:S(2)}, u32[]{:S(2)}) %collective-permute-start.4) | collective-permute-done | bytes 131104 | tf_op jit(solution)/shard_map/ppermute | solution.py:15
  53.9 8.0 %collective-permute-done.5 = bf16[128,512]{1,0:T(8,128)(2,1)S(1)} collective-permute-done((bf16[128,512]{1,0:T(8,128)(2,1)S(1)}, bf16[128,512]{1,0:T(8,128)(2,1)S(1)}, u32[]{:S(2)}, u32[]{:S(2)}) %collective-permute-start.5) | collective-permute-done | bytes 131104 | tf_op jit(solution)/shard_map/ppermute | solution.py:15
  61.9 7.7 %collective-permute-done.6 = bf16[128,512]{1,0:T(8,128)(2,1)S(1)} collective-permute-done((bf16[128,512]{1,0:T(8,128)(2,1)S(1)}, bf16[128,512]{1,0:T(8,128)(2,1)S(1)}, u32[]{:S(2)}, u32[]{:S(2)}) %collective-permute-start.6) | collective-permute-done | bytes 131104 | tf_op jit(solution)/shard_map/ppermute | solution.py:15
  70.4 4.1 %convolution_convert_fusion.1 = bf16[128,768]{1,0:T(8,128)(2,1)S(1)} fusion(bf16[4096,768]{1,0:T(8,128)(2,1)} %copy-done.4, f32[4096]{0:T(1024)S(1)} %bitcast.161, f32[128]{0:T(128)S(1)} %add_rsqrt_fusion.3, s32[]{:T(128)S(6)} %select_n.56, bf16[128,4096]{1,0:T(8,128)(2,1)S(1)} %constant_dynamic-update-slice_fusion), kind=kOutput, calls=%fused_computation.52 | convolution fusion | flops 809074688 | bytes 7553540 | tf_op jit(solution)/shard_map/dot_general | solution.py:98
  78.5 3.9 all-to-all-done.4
  82.4 3.3 all-to-all-start.1
  85.8 3.7 all-to-all-done.1
  89.6 3.3 all-to-all-start.2
  92.8 3.9 all-to-all-done.2
  96.7 3.3 all-to-all-start.3
  100.0 3.9 all-to-all-done.3
  103.9 3.3 all-to-all-start
  107.4 3.7 all-to-all-done
  111.1 3.3 all-to-all-start.5
  115.6 15.4 %fusion = f32[32,8,1,64]{3,2,1,0:T(1,128)S(1)} fusion(f32[32,8,64,1]{2,3,1,0:T(1,128)S(1)} %bitcast.154, f32[2,32,8,64,64]{4,3,2,1,0:T(8,128)} %param.29), kind=kOutput, calls=%fused_computation.2 | convolution fusion | flops 12582912 | bytes 8519680 | tf_op jit(solution)/shard_map/bhij,bhj->bhi/dot_general | solution.py:46
  131.0 11.1 %fusion.4 = f32[32,8,1,64]{3,2,1,0:T(1,128)S(1)} fusion(bf16[32,8,64,1]{2,3,1,0:T(2,128)(2,1)S(1)} %reshape.317, f32[2,32,8,64,64]{4,3,2,1,0:T(8,128)} %param.29, f32[32,8,64]{2,1,0:T(8,128)S(1)} %get-tuple-element.24, f32[32,8,64]{2,1,0:T(8,128)S(1)} %reshape.299, f32[32,8,64]{2,1,0:T(8,128)S(1)} %get-tuple-element.23, f32[32,8,64]{2,1,0:T(8,128)S(1)} %bitcast.150, ...), kind=kOutput, calls=%fused_computation.7 | convolution fusion | flops 18874368 | bytes 8814624 | tf_op jit(solution)/shard_map/bhij,bhj->bhi/dot_general | solution.py:53
  142.7 5.9 %all_gather.19 = bf16[128,512]{1,0:T(8,128)(2,1)} all-gather(bf16[32,512]{1,0:T(8,128)(2,1)S(1)} %fusion.61), channel_id=1, replica_groups=mesh['tp'=8,'dp'=4] {'dp'}, dimensions={0}, use_global_device_ids=true | all-gather | bytes 163840 | tf_op jit(solution)/shard_map/all_gather | solution.py:123
  148.5 37.1 %all-gather.3.cloned.1.call-done = bf16[128,4096]{1,0:T(8,128)(2,1)} async-done(((bf16[128,512]{1,0:T(8,128)(2,1)}), bf16[128,4096]{1,0:T(8,128)(2,1)}) %all-gather.3.cloned.1.call-update) | async-done | bytes 1048592 | tf_op jit(solution)/shard_map/all_gather | solution.py:32
  187.6 6.6 %all_to_all.200 = bf16[4,32,128]{2,1,0:T(8,128)(2,1)S(1)} all-to-all(bf16[4,32,128]{2,1,0:T(8,128)(2,1)S(1)} %bitcast.159), channel_id=1, replica_groups=mesh['tp'=8,'dp'=4] {'dp'}, dimensions={0} | all-to-all | bytes 65536 | tf_op jit(solution)/shard_map/all_to_all | solution.py:132
  194.2 5.4 %all_gather.21 = bf16[128,512]{1,0:T(8,128)(2,1)S(1)} all-gather(bf16[32,512]{1,0:T(8,128)(2,1)S(1)} %copy_bitcast_fusion.1), channel_id=1, replica_groups=mesh['tp'=8,'dp'=4] {'dp'}, dimensions={0}, use_global_device_ids=true | all-gather | bytes 163840 | tf_op jit(solution)/shard_map/all_gather | solution.py:93
  200.5 7.5 %collective-permute-done.7 = bf16[128,512]{1,0:T(8,128)(2,1)S(1)} collective-permute-done((bf16[128,512]{1,0:T(8,128)(2,1)S(1)}, bf16[128,512]{1,0:T(8,128)(2,1)S(1)}, u32[]{:S(2)}, u32[]{:S(2)}) %collective-permute-start.7) | collective-permute-done | bytes 131104 | tf_op jit(solution)/shard_map/ppermute | solution.py:15
  208.0 7.7 %collective-permute-done.8 = bf16[128,512]{1,0:T(8,128)(2,1)S(1)} collective-permute-done((bf16[128,512]{1,0:T(8,128)(2,1)S(1)}, bf16[128,512]{1,0:T(8,128)(2,1)S(1)}, u32[]{:S(2)}, u32[]{:S(2)}) %collective-permute-start.8) | collective-permute-done | bytes 131104 | tf_op jit(solution)/shard_map/ppermute | solution.py:15
  215.7 7.7 %collective-permute-done.9 = bf16[128,512]{1,0:T(8,128)(2,1)S(1)} collective-permute-done((bf16[128,512]{1,0:T(8,128)(2,1)S(1)}, bf16[128,512]{1,0:T(8,128)(2,1)S(1)}, u32[]{:S(2)}, u32[]{:S(2)}) %collective-permute-start.9) | collective-permute-done | bytes 131104 | tf_op jit(solution)/shard_map/ppermute | solution.py:15
  223.4 7.7 %collective-permute-done.10 = bf16[128,512]{1,0:T(8,128)(2,1)S(1)} collective-permute-done((bf16[128,512]{1,0:T(8,128)(2,1)S(1)}, bf16[128,512]{1,0:T(8,128)(2,1)S(1)}, u32[]{:S(2)}, u32[]{:S(2)}) %collective-permute-start.10) | collective-permute-done | bytes 131104 | tf_op jit(solution)/shard_map/ppermute | solution.py:15
  231.0 7.7 %collective-permute-done.11 = bf16[128,512]{1,0:T(8,128)(2,1)S(1)} collective-permute-done((bf16[128,512]{1,0:T(8,128)(2,1)S(1)}, bf16[128,512]{1,0:T(8,128)(2,1)S(1)}, u32[]{:S(2)}, u32[]{:S(2)}) %collective-permute-start.11) | collective-permute-done | bytes 131104 | tf_op jit(solution)/shard_map/ppermute | solution.py:15
  238.7 8.6 %collective-permute-done.12 = bf16[128,512]{1,0:T(8,128)(2,1)S(1)} collective-permute-done((bf16[128,512]{1,0:T(8,128)(2,1)S(1)}, bf16[128,512]{1,0:T(8,128)(2,1)S(1)}, u32[]{:S(2)}, u32[]{:S(2)}) %collective-permute-start.12) | collective-permute-done | bytes 131104 | tf_op jit(solution)/shard_map/ppermute | solution.py:15
  247.3 7.7 %collective-permute-done.13 = bf16[128,512]{1,0:T(8,128)(2,1)S(1)} collective-permute-done((bf16[128,512]{1,0:T(8,128)(2,1)S(1)}, bf16[128,512]{1,0:T(8,128)(2,1)S(1)}, u32[]{:S(2)}, u32[]{:S(2)}) %collective-permute-start.13) | collective-permute-done | bytes 131104 | tf_op jit(solution)/shard_map/ppermute | solution.py:15
  255.8 4.1 %convolution_convert_fusion = bf16[128,768]{1,0:T(8,128)(2,1)S(1)} fusion(bf16[4096,768]{1,0:T(8,128)(2,1)} %copy-done.5, f32[4096]{0:T(1024)S(1)} %bitcast.160, f32[128]{0:T(128)S(1)} %add_rsqrt_fusion.2, s32[]{:T(128)S(6)} %select_n.56, bf16[128,4096]{1,0:T(8,128)(2,1)S(1)} %constant_dynamic-update-slice_fusion.8), kind=kOutput, calls=%fused_computation.51 | convolution fusion | flops 809074688 | bytes 7553540 | tf_op jit(solution)/shard_map/dot_general | solution.py:98
  260.6 6.3 %all_to_all.201 = bf16[4,32,128]{2,1,0:T(8,128)(2,1)S(1)} all-to-all(bf16[4,32,128]{2,1,0:T(8,128)(2,1)S(1)} %bitcast.156), channel_id=1, replica_groups=mesh['tp'=8,'dp'=4] {'dp'}, dimensions={0} | all-to-all | bytes 65536 | tf_op jit(solution)/shard_map/all_to_all | solution.py:103
  266.9 3.3 all-to-all-start.8
  270.3 3.8 all-to-all-done.8
  274.0 3.5 all-to-all-start.9
  277.6 3.9 all-to-all-done.9
  284.7 3.9 all-to-all-done.10
  288.6 3.3 all-to-all-start.7
  292.1 3.7 all-to-all-done.7
  295.8 3.3 all-to-all-start.12
  300.0 15.4 %fusion.5 = f32[32,8,1,64]{3,2,1,0:T(1,128)S(1)} fusion(f32[32,8,64,1]{2,3,1,0:T(1,128)S(1)} %bitcast.155, f32[2,32,8,64,64]{4,3,2,1,0:T(8,128)} %param.29), kind=kOutput, calls=%fused_computation.9 | convolution fusion | flops 12582912 | bytes 8519680 | tf_op jit(solution)/shard_map/bhij,bhj->bhi/dot_general | solution.py:46
  315.5 11.1 %fusion.9 = f32[32,8,1,64]{3,2,1,0:T(1,128)S(1)} fusion(bf16[32,8,64,1]{2,3,1,0:T(2,128)(2,1)S(1)} %reshape.319, f32[2,32,8,64,64]{4,3,2,1,0:T(8,128)} %param.29, f32[32,8,64]{2,1,0:T(8,128)S(1)} %get-tuple-element.22, f32[32,8,64]{2,1,0:T(8,128)S(1)} %reshape.305, f32[32,8,64]{2,1,0:T(8,128)S(1)} %get-tuple-element.21, f32[32,8,64]{2,1,0:T(8,128)S(1)} %bitcast.152, ...), kind=kOutput, calls=%fused_computation.14 | convolution fusion | flops 18874368 | bytes 8814624 | tf_op jit(solution)/shard_map/bhij,bhj->bhi/dot_general | solution.py:53
  327.2 5.9 %all_gather.22 = bf16[128,512]{1,0:T(8,128)(2,1)} all-gather(bf16[32,512]{1,0:T(8,128)(2,1)S(1)} %fusion.59), channel_id=1, replica_groups=mesh['tp'=8,'dp'=4] {'dp'}, dimensions={0}, use_global_device_ids=true | all-gather | bytes 163840 | tf_op jit(solution)/shard_map/all_gather | solution.py:123
  333.1 13.7 %add_select_fusion.1 = (f32[1,32,8,64,64]{4,3,2,1,0:T(8,128)}, f32[1,32,8,64,64]{4,3,2,1,0:T(8,128)}) fusion(f32[2,32,8,64,64]{4,3,2,1,0:T(8,128)} %param.29, f32[32,8,64]{2,1,0:T(8,128)S(1)} %get-tuple-element.24, f32[32,8,64]{2,1,0:T(8,128)S(1)} %reshape.299, f32[32,8,64]{2,1,0:T(8,128)S(1)} %get-tuple-element.23, f32[32,8,64]{2,1,0:T(8,128)S(1)} %bitcast.151, ...), kind=kLoop, calls=%fused_computation.16 | loop fusion | flops 12582912 | bytes 17432608 | tf_op jit(solution)/shard_map/jit(_where)/select_n | solution.py:52
  346.8 23.5 %all-gather.5.cloned.1.call-done = bf16[128,4096]{1,0:T(8,128)(2,1)} async-done(((bf16[128,512]{1,0:T(8,128)(2,1)}), bf16[128,4096]{1,0:T(8,128)(2,1)}) %all-gather.5.cloned.1.call-update) | async-done | bytes 1048592 | tf_op jit(solution)/shard_map/all_gather | solution.py:32
  372.9 3.3 all-to-all-start.13
  376.2 12.5 %pad_maximum_fusion = f32[2,32,8,64,64]{4,3,2,1,0:T(8,128)} fusion(f32[1,32,8,64,64]{4,3,2,1,0:T(8,128)} %get-tuple-element.8, f32[1,32,8,64,64]{4,3,2,1,0:T(8,128)} %get-tuple-element.7), kind=kLoop, calls=%fused_computation | loop fusion | flops 2097152 | bytes 16777216 | tf_op jit(solution)/shard_map/stack | solution.py:133
  (136 shorter events, 33.1 us)
Async XLA Ops:
  7.2 15.8 %copy-start = (bf16[2,4096,128]{2,1,0:T(8,128)(2,1)S(1)}, bf16[2,4096,128]{2,1,0:T(8,128)(2,1)}, u32[]{:S(2)}) copy-start(bf16[2,4096,128]{2,1,0:T(8,128)(2,1)} %param.21) | copy-start | bytes 6291460
  14.0 16.8 %copy-start.1 = (bf16[2,4096,128]{2,1,0:T(8,128)(2,1)S(1)}, bf16[2,4096,128]{2,1,0:T(8,128)(2,1)}, u32[]{:S(2)}) copy-start(bf16[2,4096,128]{2,1,0:T(8,128)(2,1)} %param.22) | copy-start | bytes 6291460
  14.0 8.9 %collective-permute-start = (bf16[128,512]{1,0:T(8,128)(2,1)S(1)}, bf16[128,512]{1,0:T(8,128)(2,1)S(1)}, u32[]{:S(2)}, u32[]{:S(2)}) collective-permute-start(bf16[128,512]{1,0:T(8,128)(2,1)S(1)} %all_gather.18), channel_id=1, source_target_pairs={{0,4},{4,8},{8,12},{12,16},{16,20},{20,24},{24,28},{28,0},{1,5},{5... | collective-permute-start | bytes 393224 | tf_op jit(solution)/shard_map/ppermute | solution.py:15
  17.8 20.7 %copy-start.2 = (bf16[2,4096,128]{2,1,0:T(8,128)(2,1)S(1)}, bf16[2,4096,128]{2,1,0:T(8,128)(2,1)}, u32[]{:S(2)}) copy-start(bf16[2,4096,128]{2,1,0:T(8,128)(2,1)} %param.23) | copy-start | bytes 6291460
  23.0 7.9 %collective-permute-start.1 = (bf16[128,512]{1,0:T(8,128)(2,1)S(1)}, bf16[128,512]{1,0:T(8,128)(2,1)S(1)}, u32[]{:S(2)}, u32[]{:S(2)}) collective-permute-start(bf16[128,512]{1,0:T(8,128)(2,1)S(1)} %collective-permute-done), channel_id=1, source_target_pairs={{0,4},{4,8},{8,12},{12,16},{16,20},{20,24},{24,28},{28,0},{1,5},{5... | collective-permute-start | bytes 393224 | tf_op jit(solution)/shard_map/ppermute | solution.py:15
  23.0 23.2 %copy-start.3 = (bf16[2,4096,128]{2,1,0:T(8,128)(2,1)S(1)}, bf16[2,4096,128]{2,1,0:T(8,128)(2,1)}, u32[]{:S(2)}) copy-start(bf16[2,4096,128]{2,1,0:T(8,128)(2,1)} %param.24) | copy-start | bytes 6291460
  30.8 7.7 %collective-permute-start.2 = (bf16[128,512]{1,0:T(8,128)(2,1)S(1)}, bf16[128,512]{1,0:T(8,128)(2,1)S(1)}, u32[]{:S(2)}, u32[]{:S(2)}) collective-permute-start(bf16[128,512]{1,0:T(8,128)(2,1)S(1)} %collective-permute-done.1), channel_id=1, source_target_pairs={{0,4},{4,8},{8,12},{12,16},{16,20},{20,24},{24,28},{28,0},{1,5},{5... | collective-permute-start | bytes 393224 | tf_op jit(solution)/shard_map/ppermute | solution.py:15
  30.9 23.0 %copy-start.6 = (f32[2,4096]{1,0:T(2,128)S(1)}, f32[2,4096]{1,0:T(2,128)}, u32[]{:S(2)}) copy-start(f32[2,4096]{1,0:T(2,128)} %param.18) | copy-start | bytes 98308
  30.9 31.0 %copy-start.7 = (f32[2,512]{1,0:T(2,128)S(1)}, f32[2,512]{1,0:T(2,128)}, u32[]{:S(2)}) copy-start(f32[2,512]{1,0:T(2,128)} %param.28) | copy-start | bytes 12292
  38.5 7.7 %collective-permute-start.3 = (bf16[128,512]{1,0:T(8,128)(2,1)S(1)}, bf16[128,512]{1,0:T(8,128)(2,1)S(1)}, u32[]{:S(2)}, u32[]{:S(2)}) collective-permute-start(bf16[128,512]{1,0:T(8,128)(2,1)S(1)} %collective-permute-done.2), channel_id=1, source_target_pairs={{0,4},{4,8},{8,12},{12,16},{16,20},{20,24},{24,28},{28,0},{1,5},{5... | collective-permute-start | bytes 393224 | tf_op jit(solution)/shard_map/ppermute | solution.py:15
  46.2 7.7 %collective-permute-start.4 = (bf16[128,512]{1,0:T(8,128)(2,1)S(1)}, bf16[128,512]{1,0:T(8,128)(2,1)S(1)}, u32[]{:S(2)}, u32[]{:S(2)}) collective-permute-start(bf16[128,512]{1,0:T(8,128)(2,1)S(1)} %collective-permute-done.3), channel_id=1, source_target_pairs={{0,4},{4,8},{8,12},{12,16},{16,20},{20,24},{24,28},{28,0},{1,5},{5... | collective-permute-start | bytes 393224 | tf_op jit(solution)/shard_map/ppermute | solution.py:15
  46.7 2.6 copy-start.4
  49.3 4.5 %copy-start.5 = (bf16[4096,768]{1,0:T(8,128)(2,1)}, bf16[4096,768]{1,0:T(8,128)(2,1)S(1)}, u32[]{:S(2)}) copy-start(bf16[4096,768]{1,0:T(8,128)(2,1)S(1)} %get-tuple-element.10) | copy-start | bytes 18874372
  53.8 8.1 %collective-permute-start.5 = (bf16[128,512]{1,0:T(8,128)(2,1)S(1)}, bf16[128,512]{1,0:T(8,128)(2,1)S(1)}, u32[]{:S(2)}, u32[]{:S(2)}) collective-permute-start(bf16[128,512]{1,0:T(8,128)(2,1)S(1)} %collective-permute-done.4), channel_id=1, source_target_pairs={{0,4},{4,8},{8,12},{12,16},{16,20},{20,24},{24,28},{28,0},{1,5},{5... | collective-permute-start | bytes 393224 | tf_op jit(solution)/shard_map/ppermute | solution.py:15
  61.9 7.7 %collective-permute-start.6 = (bf16[128,512]{1,0:T(8,128)(2,1)S(1)}, bf16[128,512]{1,0:T(8,128)(2,1)S(1)}, u32[]{:S(2)}, u32[]{:S(2)}) collective-permute-start(bf16[128,512]{1,0:T(8,128)(2,1)S(1)} %collective-permute-done.5), channel_id=1, source_target_pairs={{0,4},{4,8},{8,12},{12,16},{16,20},{20,24},{24,28},{28,0},{1,5},{5... | collective-permute-start | bytes 393224 | tf_op jit(solution)/shard_map/ppermute | solution.py:15
  69.6 8.8 %copy-start.10 = (s32[32]{0:T(128)S(1)}, s32[32]{0:T(128)}, u32[]{:S(2)}) copy-start(s32[32]{0:T(128)} %param.17) | copy-start | bytes 388
  69.6 16.0 %copy-start.8 = (f32[2,512]{1,0:T(2,128)S(1)}, f32[2,512]{1,0:T(2,128)}, u32[]{:S(2)}) copy-start(f32[2,512]{1,0:T(2,128)} %param.27) | copy-start | bytes 12292
  69.6 16.0 %copy-start.9 = (f32[2,512]{1,0:T(2,128)S(1)}, f32[2,512]{1,0:T(2,128)}, u32[]{:S(2)}) copy-start(f32[2,512]{1,0:T(2,128)} %param.26) | copy-start | bytes 12292
  75.2 7.2 %all-to-all-start.4 = ((bf16[4,32,128]{2,1,0:T(8,128)(2,1)}), bf16[4,32,128]{2,1,0:T(8,128)(2,1)S(1)}, u32[]{:S(2)}, u32[]{:S(2)}) async-start(bf16[4,32,128]{2,1,0:T(8,128)(2,1)} %bitcast.21), calls=%async_computation.4 | async-start | bytes 65536 | tf_op jit(solution)/shard_map/all_to_all | solution.py:103
  82.4 7.2 %all-to-all-start.1 = ((bf16[4,32,128]{2,1,0:T(8,128)(2,1)}), bf16[4,32,128]{2,1,0:T(8,128)(2,1)S(1)}, u32[]{:S(2)}, u32[]{:S(2)}) async-start(bf16[4,32,128]{2,1,0:T(8,128)(2,1)} %bitcast.11), calls=%async_computation.1 | async-start | bytes 65536 | tf_op jit(solution)/shard_map/all_to_all | solution.py:104
  89.6 7.2 %all-to-all-start.2 = ((bf16[4,32,128]{2,1,0:T(8,128)(2,1)}), bf16[4,32,128]{2,1,0:T(8,128)(2,1)S(1)}, u32[]{:S(2)}, u32[]{:S(2)}) async-start(bf16[4,32,128]{2,1,0:T(8,128)(2,1)} %bitcast.17), calls=%async_computation.2 | async-start | bytes 65536 | tf_op jit(solution)/shard_map/all_to_all | solution.py:107
  96.7 7.2 %all-to-all-start.3 = ((bf16[4,32,128]{2,1,0:T(8,128)(2,1)}), bf16[4,32,128]{2,1,0:T(8,128)(2,1)S(1)}, u32[]{:S(2)}, u32[]{:S(2)}) async-start(bf16[4,32,128]{2,1,0:T(8,128)(2,1)} %bitcast.19), calls=%async_computation.3 | async-start | bytes 65536 | tf_op jit(solution)/shard_map/all_to_all | solution.py:105
  103.9 7.2 %all-to-all-start = ((bf16[4,32,128]{2,1,0:T(8,128)(2,1)}), bf16[4,32,128]{2,1,0:T(8,128)(2,1)S(1)}, u32[]{:S(2)}, u32[]{:S(2)}) async-start(bf16[4,32,128]{2,1,0:T(8,128)(2,1)} %bitcast.9), calls=%async_computation | async-start | bytes 65536 | tf_op jit(solution)/shard_map/all_to_all | solution.py:106
  111.1 31.5 %all-to-all-start.5 = ((bf16[4,32,128]{2,1,0:T(8,128)(2,1)}), bf16[4,32,128]{2,1,0:T(8,128)(2,1)S(1)}, u32[]{:S(2)}, u32[]{:S(2)}) async-start(bf16[4,32,128]{2,1,0:T(8,128)(2,1)} %bitcast.26), calls=%async_computation.5 | async-start | bytes 65536 | tf_op jit(solution)/shard_map/all_to_all | solution.py:108
  114.4 71.2 %all-gather.3.cloned.1.call-start = ((), (), s32[]{:S(2)}) async-start(), calls=%async_computation.14 | async-start | bytes 1179648 | tf_op jit(solution)/shard_map/all_gather | solution.py:32
  199.6 8.4 %collective-permute-start.7 = (bf16[128,512]{1,0:T(8,128)(2,1)S(1)}, bf16[128,512]{1,0:T(8,128)(2,1)S(1)}, u32[]{:S(2)}, u32[]{:S(2)}) collective-permute-start(bf16[128,512]{1,0:T(8,128)(2,1)S(1)} %all_gather.21), channel_id=1, source_target_pairs={{0,4},{4,8},{8,12},{12,16},{16,20},{20,24},{24,28},{28,0},{1,5},{5... | collective-permute-start | bytes 393224 | tf_op jit(solution)/shard_map/ppermute | solution.py:15
  208.0 7.7 %collective-permute-start.8 = (bf16[128,512]{1,0:T(8,128)(2,1)S(1)}, bf16[128,512]{1,0:T(8,128)(2,1)S(1)}, u32[]{:S(2)}, u32[]{:S(2)}) collective-permute-start(bf16[128,512]{1,0:T(8,128)(2,1)S(1)} %collective-permute-done.7), channel_id=1, source_target_pairs={{0,4},{4,8},{8,12},{12,16},{16,20},{20,24},{24,28},{28,0},{1,5},{5... | collective-permute-start | bytes 393224 | tf_op jit(solution)/shard_map/ppermute | solution.py:15
  215.7 7.7 %collective-permute-start.9 = (bf16[128,512]{1,0:T(8,128)(2,1)S(1)}, bf16[128,512]{1,0:T(8,128)(2,1)S(1)}, u32[]{:S(2)}, u32[]{:S(2)}) collective-permute-start(bf16[128,512]{1,0:T(8,128)(2,1)S(1)} %collective-permute-done.8), channel_id=1, source_target_pairs={{0,4},{4,8},{8,12},{12,16},{16,20},{20,24},{24,28},{28,0},{1,5},{5... | collective-permute-start | bytes 393224 | tf_op jit(solution)/shard_map/ppermute | solution.py:15
  223.4 7.7 %collective-permute-start.10 = (bf16[128,512]{1,0:T(8,128)(2,1)S(1)}, bf16[128,512]{1,0:T(8,128)(2,1)S(1)}, u32[]{:S(2)}, u32[]{:S(2)}) collective-permute-start(bf16[128,512]{1,0:T(8,128)(2,1)S(1)} %collective-permute-done.9), channel_id=1, source_target_pairs={{0,4},{4,8},{8,12},{12,16},{16,20},{20,24},{24,28},{28,0},{1,5},{5... | collective-permute-start | bytes 393224 | tf_op jit(solution)/shard_map/ppermute | solution.py:15
  231.0 7.7 %collective-permute-start.11 = (bf16[128,512]{1,0:T(8,128)(2,1)S(1)}, bf16[128,512]{1,0:T(8,128)(2,1)S(1)}, u32[]{:S(2)}, u32[]{:S(2)}) collective-permute-start(bf16[128,512]{1,0:T(8,128)(2,1)S(1)} %collective-permute-done.10), channel_id=1, source_target_pairs={{0,4},{4,8},{8,12},{12,16},{16,20},{20,24},{24,28},{28,0},{1,5},{5... | collective-permute-start | bytes 393224 | tf_op jit(solution)/shard_map/ppermute | solution.py:15
  238.7 8.6 %collective-permute-start.12 = (bf16[128,512]{1,0:T(8,128)(2,1)S(1)}, bf16[128,512]{1,0:T(8,128)(2,1)S(1)}, u32[]{:S(2)}, u32[]{:S(2)}) collective-permute-start(bf16[128,512]{1,0:T(8,128)(2,1)S(1)} %collective-permute-done.11), channel_id=1, source_target_pairs={{0,4},{4,8},{8,12},{12,16},{16,20},{20,24},{24,28},{28,0},{1,5},{5... | collective-permute-start | bytes 393224 | tf_op jit(solution)/shard_map/ppermute | solution.py:15
  247.3 7.7 %collective-permute-start.13 = (bf16[128,512]{1,0:T(8,128)(2,1)S(1)}, bf16[128,512]{1,0:T(8,128)(2,1)S(1)}, u32[]{:S(2)}, u32[]{:S(2)}) collective-permute-start(bf16[128,512]{1,0:T(8,128)(2,1)S(1)} %collective-permute-done.12), channel_id=1, source_target_pairs={{0,4},{4,8},{8,12},{12,16},{16,20},{20,24},{24,28},{28,0},{1,5},{5... | collective-permute-start | bytes 393224 | tf_op jit(solution)/shard_map/ppermute | solution.py:15
  266.9 7.2 %all-to-all-start.8 = ((bf16[4,32,128]{2,1,0:T(8,128)(2,1)}), bf16[4,32,128]{2,1,0:T(8,128)(2,1)S(1)}, u32[]{:S(2)}, u32[]{:S(2)}) async-start(bf16[4,32,128]{2,1,0:T(8,128)(2,1)} %bitcast.40), calls=%async_computation.8 | async-start | bytes 65536 | tf_op jit(solution)/shard_map/all_to_all | solution.py:104
  274.0 7.4 %all-to-all-start.9 = ((bf16[4,32,128]{2,1,0:T(8,128)(2,1)}), bf16[4,32,128]{2,1,0:T(8,128)(2,1)S(1)}, u32[]{:S(2)}, u32[]{:S(2)}) async-start(bf16[4,32,128]{2,1,0:T(8,128)(2,1)} %bitcast.46), calls=%async_computation.9 | async-start | bytes 65536 | tf_op jit(solution)/shard_map/all_to_all | solution.py:107
  281.4 7.2 %all-to-all-start.10 = ((bf16[4,32,128]{2,1,0:T(8,128)(2,1)}), bf16[4,32,128]{2,1,0:T(8,128)(2,1)S(1)}, u32[]{:S(2)}, u32[]{:S(2)}) async-start(bf16[4,32,128]{2,1,0:T(8,128)(2,1)} %bitcast.48), calls=%async_computation.10 | async-start | bytes 65536 | tf_op jit(solution)/shard_map/all_to_all | solution.py:105
  288.6 7.2 %all-to-all-start.7 = ((bf16[4,32,128]{2,1,0:T(8,128)(2,1)}), bf16[4,32,128]{2,1,0:T(8,128)(2,1)S(1)}, u32[]{:S(2)}, u32[]{:S(2)}) async-start(bf16[4,32,128]{2,1,0:T(8,128)(2,1)} %bitcast.38), calls=%async_computation.7 | async-start | bytes 65536 | tf_op jit(solution)/shard_map/all_to_all | solution.py:106
  295.8 31.3 %all-to-all-start.12 = ((bf16[4,32,128]{2,1,0:T(8,128)(2,1)}), bf16[4,32,128]{2,1,0:T(8,128)(2,1)S(1)}, u32[]{:S(2)}, u32[]{:S(2)}) async-start(bf16[4,32,128]{2,1,0:T(8,128)(2,1)} %bitcast.55), calls=%async_computation.12 | async-start | bytes 65536 | tf_op jit(solution)/shard_map/all_to_all | solution.py:108
  299.1 71.2 %all-gather.5.cloned.1.call-start = ((), (), s32[]{:S(2)}) async-start(), calls=%async_computation.15 | async-start | bytes 1179648 | tf_op jit(solution)/shard_map/all_gather | solution.py:32
  372.9 15.8 %all-to-all-start.13 = ((bf16[4,32,128]{2,1,0:T(8,128)(2,1)}), bf16[4,32,128]{2,1,0:T(8,128)(2,1)S(1)}, u32[]{:S(2)}, u32[]{:S(2)}) async-start(bf16[4,32,128]{2,1,0:T(8,128)(2,1)} %bitcast.58), calls=%async_computation.13 | async-start | bytes 65536 | tf_op jit(solution)/shard_map/all_to_all | solution.py:132
Sparse Core Ops, SparseCore 0:
  148.7 36.9 all-gather.2
  333.2 37.0 all-gather.4
